TPU v7x, 32 devices: a whole 2x2x4 slice. The times are simulated.
32 devices in a mesh: sp: 8 (over z, x), dp: 4 (over y, core).
Axes of the slice: x: 2, y: 2, z: 4, core: 2. Of those that a mesh axis runs over, the one named last changes fastest.
Arguments:
- inputs: bfloat16 [4, 2048, 2048], P('dp', 'sp'), may hold values from -6 to 6
- up_pre: bfloat16 [4, 2048, 1024], P('dp', 'sp'), may hold values from -6 to 6
- gate_pre: bfloat16 [4, 2048, 1024], P('dp', 'sp'), may hold values from -6 to 6
- cotangent: bfloat16 [4, 2048, 1024], P('dp', 'sp'), may hold values from -6 to 6
- norm_gain: float32 [1024], replicated, may hold values from 0.1 to 1.9
- up_weight: bfloat16 [2048, 1024], P('dp'), may hold values from -0.125 to 0.125
- gate_weight: bfloat16 [2048, 1024], P('dp'), may hold values from -0.125 to 0.125
- mix_weight: bfloat16 [8, 512, 512], replicated, may hold values from -0.375 to 0.375
Outputs:
- input_grad: bfloat16 [4, 2048, 2048], P('dp', 'sp')
- up_weight_grad: float32 [2048, 1024], P('dp')
- gate_weight_grad: float32 [2048, 1024], P('dp')
All inputs are finite; a program needn't handle non-finite values.
Results may differ from a plain program's by a relative error of at most 0.0064.
Values may be sent and summed in bfloat16 or wider, within the bound.
No kernel may reach another device: no remote copies, remote signals or barrier semaphores. Data moves between devices by JAX's collectives and lax.ppermute only.
A program may use at most 128 MiB of HBM per device.

v0:
```python
import math

import jax
import jax.numpy as jnp
from jax import lax
from jax.sharding import PartitionSpec as P

GROUP_CH = 128
SPAN = 512
SEG = 64


norm_eps = 1e-05
grad_scale = 1.0 / 256.0
root_half = 1.0 / math.sqrt(2.0)
root_twopi = 1.0 / math.sqrt(2.0 * math.pi)


def gelu_value(preact):
    return 0.5 * preact * (1.0 + lax.erf(preact * root_half))


def gelu_slope(preact):
    return (
        0.5 * (1.0 + lax.erf(preact * root_half))
        + preact * jnp.exp(-0.5 * preact * preact) * root_twopi
    )


def span_mask():
    segment = jnp.arange(SPAN) // SEG
    return segment[None, :] <= segment[:, None]


def contract(first_op, second_op):
    return lax.dot_general(
        first_op, second_op, (((1,), (1,)), ((), ())), preferred_element_type=jnp.float32
    )


def on_device(inputs, up_pre, gate_pre, cotangent, norm_gain, up_weight, gate_weight, mix_weight):
    sequences, own_rows, gated_width = cotangent.shape
    model_width = inputs.shape[2]
    up_float = up_pre.astype(jnp.float32)
    gate_float = gate_pre.astype(jnp.float32)
    grad_float = cotangent.astype(jnp.float32)
    gated_act = gelu_value(gate_float)
    centered = gated_act - jnp.mean(gated_act, axis=-1, keepdims=True)
    inverse_std = lax.rsqrt(jnp.mean(centered * centered, axis=-1, keepdims=True) + norm_eps)
    normed = centered * inverse_std
    mixer_in = (normed * norm_gain).astype(jnp.bfloat16)
    mixer_grad = (grad_float * gelu_value(up_float)).astype(jnp.bfloat16)
    arrived = (
        lax.all_to_all(mixer_grad, "sp", split_axis=2, concat_axis=1, tiled=True),
        lax.all_to_all(mixer_in, "sp", split_axis=2, concat_axis=1, tiled=True),
    )
    channels = arrived[0].shape[2]
    group_index = lax.axis_index("sp") * channels // GROUP_CH
    weight_group = lax.dynamic_index_in_dim(mix_weight, group_index, 0, keepdims=False)
    masked = jnp.where(span_mask(), weight_group, jnp.zeros_like(weight_group))
    grad_blocks = arrived[0].reshape(-1, SPAN, channels)
    input_blocks = arrived[1].reshape(-1, SPAN, channels)
    spatial = jnp.einsum(
        "ts,nsc->ntc", masked, input_blocks, preferred_element_type=jnp.float32
    ).astype(jnp.bfloat16)
    normed_back = jnp.einsum(
        "ts,ntc->nsc", masked, grad_blocks, preferred_element_type=jnp.float32
    ).astype(jnp.bfloat16)
    returned = (
        lax.all_to_all(
            spatial.reshape(sequences, -1, channels), "sp", split_axis=1, concat_axis=2, tiled=True
        ),
        lax.all_to_all(
            normed_back.reshape(sequences, -1, channels),
            "sp",
            split_axis=1,
            concat_axis=2,
            tiled=True,
        ),
    )
    spatial_tokens = returned[0]
    back_tokens = returned[1]
    up_pre_grad = (grad_float * spatial_tokens.astype(jnp.float32) * gelu_slope(up_float)).astype(
        jnp.bfloat16
    )
    scaled = back_tokens.astype(jnp.float32) * norm_gain
    gated_grad = inverse_std * (
        scaled
        - jnp.mean(scaled, axis=-1, keepdims=True)
        - normed * jnp.mean(scaled * normed, axis=-1, keepdims=True)
    )
    gate_pre_grad = (gated_grad * gelu_slope(gate_float)).astype(jnp.bfloat16)
    flat_up = up_pre_grad.reshape(-1, gated_width)
    flat_gate = gate_pre_grad.reshape(-1, gated_width)
    token_count = flat_up.shape[0]
    dp_count = lax.axis_size("dp")
    sp_count = lax.axis_size("sp")
    result_part = (
        contract(flat_up, lax.all_gather(up_weight, "dp", axis=0, tiled=True))
        + contract(flat_gate, lax.all_gather(gate_weight, "dp", axis=0, tiled=True))
    ).astype(jnp.bfloat16)
    input_grad = result_part.reshape(sequences, own_rows, model_width)
    flat_inputs = inputs.reshape(-1, model_width)
    both_grads = jnp.concatenate([flat_up, flat_gate], axis=1)
    row_share = model_width // (sp_count * dp_count)
    permuted = flat_inputs.reshape(token_count, dp_count, sp_count, row_share)
    permuted = permuted.transpose(0, 2, 1, 3).reshape(token_count, model_width)
    own_part = lax.psum_scatter(
        lax.dot_general(
            permuted, both_grads, (((0,), (0,)), ((), ())), preferred_element_type=jnp.float32
        ),
        ("sp", "dp"),
        scatter_dimension=0,
        tiled=True,
    )
    weight_rows = lax.all_gather(own_part, "sp", axis=0, tiled=True)
    up_weight_grad = weight_rows[:, :gated_width] * grad_scale
    gate_weight_grad = weight_rows[:, gated_width:] * grad_scale
    return (input_grad, up_weight_grad, gate_weight_grad)


def solution(mesh):
    return jax.shard_map(
        on_device,
        mesh=mesh,
        in_specs=(
            P("dp", "sp", None),
            P("dp", "sp", None),
            P("dp", "sp", None),
            P("dp", "sp", None),
            P(),
            P("dp", None),
            P("dp", None),
            P(),
        ),
        out_specs=(P("dp", "sp", None), P("dp", None), P("dp", None)),
        check_vma=False,
    )
```

profile of v0, /device:TPU:0, one launch (start us, length us, event | category | flops | bytes accessed | tf_op | source)
XLA Modules:
  0.0 505.7 jit_solution(16661399737685429163)
XLA Ops:
  8.0 1.2 copy.45
  9.2 1.2 copy.36
  10.5 0.3 fusion.6
  10.8 0.8 copy.68
  11.6 0.5 broadcast.266
  12.1 3.7 reduce.6
  15.9 0.9 reshape.291
  16.8 7.6 %all-to-all-start.2 = ((bf16[8,2,16384]{2,1,0:T(2,128)(2,1)}), bf16[8,2,16384]{2,1,0:T(2,128)(2,1)S(1)}, u32[]{:S(2)}, u32[]{:S(2)}) async-start(bf16[8,2,16384]{2,1,0:T(2,128)(2,1)} %reshape.291), calls=%async_computation.2 | async-start | bytes 1048576 | tf_op jit(solution)/shard_map/all_to_all | solution.py:54
  24.4 14.4 %all-to-all-done.2 = bf16[8,2,16384]{2,1,0:T(2,128)(2,1)S(1)} async-done(((bf16[8,2,16384]{2,1,0:T(2,128)(2,1)}), bf16[8,2,16384]{2,1,0:T(2,128)(2,1)S(1)}, u32[]{:S(2)}, u32[]{:S(2)}) %all-to-all-start.2) | async-done | bytes 524320 | tf_op jit(solution)/shard_map/all_to_all | solution.py:54
  38.8 0.5 reshape.292
  39.8 1.6 fusion.3
  41.7 8.1 %copy.67 = bf16[1,2048,128]{2,0,1:T(2,128)(2,1)S(1)} copy(bf16[1,2048,128]{2,1,0:T(8,128)(2,1)S(1)} %bitcast.88) | data formatting | bytes 1048576 | tf_op jit(solution)/shard_map/reshape | solution.py:74
  49.8 11.4 %reduce.7 = bf16[2048,128]{1,0:T(8,128)(2,1)S(1)} reduce(bf16[2048,1,128]{2,1,0:T(2,128)(2,1)S(1)} %bitcast.80, bf16[]{:T(256)} %broadcast.266), dimensions={1}, to_apply=%bitcast.69.reduce_sub_computation | reduce | bytes 1048578
  61.3 0.9 reshape.293
  62.2 4.7 all-to-all-start.3
  67.6 13.5 %all-to-all-done.3 = bf16[8,2,16384]{2,1,0:T(2,128)(2,1)} async-done(((bf16[8,2,16384]{2,1,0:T(2,128)(2,1)}), bf16[8,2,16384]{2,1,0:T(2,128)(2,1)}, u32[]{:S(2)}, u32[]{:S(2)}) %all-to-all-start.3) | async-done | bytes 524320 | tf_op jit(solution)/shard_map/all_to_all | solution.py:73
  81.1 2.2 reshape.294
  83.4 1.3 convert_bitcast_fusion
  84.6 1.6 copy.52
  86.2 1.2 fusion.7
  87.4 0.3 multiply_reduce_fusion
  87.8 1.5 fusion.15
  89.3 0.8 copy.70
  90.1 3.7 reduce.8
  94.0 18.2 %all_to_all.48 = bf16[8,2,16384]{2,1,0:T(2,128)(2,1)S(1)} all-to-all(bf16[8,2,16384]{2,1,0:T(2,128)(2,1)S(1)} %reshape.287), channel_id=1, replica_groups=mesh['sp'=8,'dp'=4] {'sp'}, dimensions={0} | all-to-all | bytes 1048576 | tf_op jit(solution)/shard_map/all_to_all | solution.py:55
  112.2 0.5 reshape.288
  112.8 0.3 copy.39
  113.1 1.6 fusion.2
  115.0 8.1 %copy.69 = bf16[1,2048,128]{2,0,1:T(2,128)(2,1)S(1)} copy(bf16[1,2048,128]{2,1,0:T(8,128)(2,1)S(1)} %bitcast.90) | data formatting | bytes 1048576 | tf_op jit(solution)/shard_map/reshape | solution.py:71
  123.1 11.4 %reduce.9 = bf16[2048,128]{1,0:T(8,128)(2,1)S(1)} reduce(bf16[2048,1,128]{2,1,0:T(2,128)(2,1)S(1)} %bitcast.79, bf16[]{:T(256)} %broadcast.266), dimensions={1}, to_apply=%bitcast.71.reduce_sub_computation | reduce | bytes 1048578
  134.6 0.9 reshape.289
  135.5 4.1 all-to-all-start.1
  139.9 1.5 copy.53
  141.5 11.9 %all-to-all-done.1 = bf16[8,2,16384]{2,1,0:T(2,128)(2,1)} async-done(((bf16[8,2,16384]{2,1,0:T(2,128)(2,1)}), bf16[8,2,16384]{2,1,0:T(2,128)(2,1)}, u32[]{:S(2)}, u32[]{:S(2)}) %all-to-all-start.1) | async-done | bytes 524320 | tf_op jit(solution)/shard_map/all_to_all | solution.py:70
  153.4 2.2 reshape.290
  155.7 1.0 convert_bitcast_fusion.1
  156.7 1.6 copy.44
  158.3 0.5 fusion.5
  158.9 0.8 copy-done.3
  159.6 9.1 %convolution_bitcast_fusion = f32[2048,2048]{0,1:T(8,128)} fusion(bf16[256,2048]{0,1:T(8,128)(2,1)S(1)} %bitcast.73, bf16[256,1024]{0,1:T(8,128)(2,1)} %bitcast.83, bf16[256,1024]{0,1:T(8,128)(2,1)S(1)} %bitcast.84), kind=kOutput, calls=%fused_computation | convolution fusion | flops 2149580800 | bytes 18874368 | tf_op jit(solution)/shard_map/dot_general | solution.py:109
  168.8 17.6 %copy.58 = f32[2048,2048]{1,0:T(8,128)} copy(f32[2048,2048]{0,1:T(8,128)} %convolution_bitcast_fusion) | data formatting | bytes 33554432
  186.4 0.5 all-gather.4.cloned.1.call-update
  187.0 0.5 all-gather.6.cloned.1.call-update
  187.6 231.8 %reduce-scatter.4.cloned.1.call-done = f32[64,2048]{1,0:T(8,128)} async-done(((f32[2048,2048]{1,0:T(8,128)}), f32[64,2048]{1,0:T(8,128)}) %reduce-scatter.4.cloned.1.call-update) | async-done | bytes 524304 | tf_op jit(solution)/shard_map/reduce_scatter | solution.py:108
  419.5 3.5 fusion.36
  423.0 4.5 fusion.1
  427.5 65.3 %all-gather.8.cloned.1.call-done = f32[512,2048]{1,0:T(8,128)} async-done(((f32[64,2048]{1,0:T(8,128)}), f32[512,2048]{1,0:T(8,128)}) %all-gather.8.cloned.1.call-update) | async-done | bytes 4194320 | tf_op jit(solution)/shard_map/all_gather | solution.py:116
  492.8 5.1 %slice_multiply_fusion = (f32[512,1024]{1,0:T(8,128)}, f32[512,1024]{1,0:T(8,128)}) fusion(f32[512,2048]{1,0:T(8,128)} %all-gather.8.cloned.1.call-done), kind=kLoop, calls=%fused_computation.4 | loop fusion | flops 1048576 | bytes 8388608 | tf_op jit(solution)/shard_map/mul | solution.py:118
  (36 shorter events, 2.5 us)
Async XLA Ops:
  10.5 28.9 %copy-start = (bf16[1,256,1024]{1,2,0:T(8,128)(2,1)}, bf16[1,256,1024]{1,2,0:T(8,128)(2,1)S(1)}, u32[]{:S(2)}) copy-start(bf16[1,256,1024]{1,2,0:T(8,128)(2,1)S(1)} %copy.36) | copy-start | bytes 1572868
  16.8 22.0 %all-to-all-start.2 = ((bf16[8,2,16384]{2,1,0:T(2,128)(2,1)}), bf16[8,2,16384]{2,1,0:T(2,128)(2,1)S(1)}, u32[]{:S(2)}, u32[]{:S(2)}) async-start(bf16[8,2,16384]{2,1,0:T(2,128)(2,1)} %reshape.291), calls=%async_computation.2 | async-start | bytes 1048576 | tf_op jit(solution)/shard_map/all_to_all | solution.py:54
  39.8 27.1 %copy-start.5 = (bf16[1,256,1024]{2,1,0:T(8,128)(2,1)S(1)}, bf16[1,256,1024]{2,1,0:T(8,128)(2,1)}, u32[]{:S(2)}) copy-start(bf16[1,256,1024]{2,1,0:T(8,128)(2,1)} %param.10) | copy-start | bytes 1572868
  62.2 18.9 %all-to-all-start.3 = ((bf16[8,2,16384]{2,1,0:T(2,128)(2,1)}), bf16[8,2,16384]{2,1,0:T(2,128)(2,1)}, u32[]{:S(2)}, u32[]{:S(2)}) async-start(bf16[8,2,16384]{2,1,0:T(2,128)(2,1)} %reshape.293), calls=%async_computation.3 | async-start | bytes 1048576 | tf_op jit(solution)/shard_map/all_to_all | solution.py:73
  67.4 18.8 %copy-start.6 = (f32[1024]{0:T(1024)S(1)}, f32[1024]{0:T(1024)}, u32[]{:S(2)}) copy-start(f32[1024]{0:T(1024)} %param.12) | copy-start | bytes 12292
  135.5 17.9 %all-to-all-start.1 = ((bf16[8,2,16384]{2,1,0:T(2,128)(2,1)}), bf16[8,2,16384]{2,1,0:T(2,128)(2,1)}, u32[]{:S(2)}, u32[]{:S(2)}) async-start(bf16[8,2,16384]{2,1,0:T(2,128)(2,1)} %reshape.289), calls=%async_computation.1 | async-start | bytes 1048576 | tf_op jit(solution)/shard_map/all_to_all | solution.py:70
  139.6 279.8 %reduce-scatter.4.cloned.1.call-start = ((), (), s32[]{:S(2)}) async-start(), calls=%async_computation.8 | async-start | bytes 17301504 | tf_op jit(solution)/shard_map/reduce_scatter | solution.py:108
  141.4 16.9 %copy-start.1 = (bf16[1,256,1024]{1,2,0:T(8,128)(2,1)S(1)}, bf16[1,256,1024]{1,2,0:T(8,128)(2,1)}, u32[]{:S(2)}) copy-start(bf16[1,256,1024]{1,2,0:T(8,128)(2,1)} %copy-done) | copy-start | bytes 1572868
  158.8 0.8 copy-start.3
  186.4 233.1 %copy-start.4 = (bf16[1,256,1024]{1,2,0:T(8,128)(2,1)S(1)}, bf16[1,256,1024]{1,2,0:T(8,128)(2,1)}, u32[]{:S(2)}) copy-start(bf16[1,256,1024]{1,2,0:T(8,128)(2,1)} %copy-done.3) | copy-start | bytes 1572868
  186.4 233.1 %all-gather.4.cloned.1.call-start = ((), (), s32[]{:S(2)}) async-start(), calls=%async_computation.5 | async-start | bytes 5242880 | tf_op jit(solution)/shard_map/all_gather | solution.py:99
  187.0 236.0 %copy-start.2 = (bf16[1,256,1024]{1,2,0:T(8,128)(2,1)S(1)}, bf16[1,256,1024]{1,2,0:T(8,128)(2,1)}, u32[]{:S(2)}) copy-start(bf16[1,256,1024]{1,2,0:T(8,128)(2,1)} %get-tuple-element.18) | copy-start | bytes 1572868
  187.0 236.0 %all-gather.6.cloned.1.call-start = ((), (), s32[]{:S(2)}) async-start(), calls=%async_computation.6 | async-start | bytes 5242880 | tf_op jit(solution)/shard_map/all_gather | solution.py:100
  187.6 305.2 %all-gather.8.cloned.1.call-start = ((), (), s32[]{:S(2)}) async-start(), calls=%async_computation.7 | async-start | bytes 4718592 | tf_op jit(solution)/shard_map/all_gather | solution.py:116
Sparse Core Ops, SparseCore 0:
  186.5 232.8 reduce-scatter.3
Sparse Core Ops, SparseCore 1:
  188.4 42.2 all-gather.3
  232.1 41.9 all-gather.5
  419.5 73.2 all-gather.7
where the time goes:
time: 511 us; the launch traced here: 506 us
  waiting for transfers between devices  338 us (66%)
  local copies, waits for them, and re-layouts  53.9 us (11%)
  other arithmetic  42.2 us (8%)
  matrix products  20.4 us (4%)
  blocking collectives  18.2 us (4%)
  starting transfers between devices  16.8 us (3%)
  between operations  16.3 us (3%)
    reduce_scatter x1, waiting for transfers between devices, on_device(): lax.psum_scatter(lax.dot_general(permuted, both_grads, (((0,), (0,)), (()...  232 us
    all_gather x1, waiting for transfers between devices, on_device(): weight_rows = lax.all_gather(own_part, 'sp', axis=0, tiled=True)  65.3 us
    unnamed x30, local copies, waits for them, and re-layouts  31.6 us
    unnamed x4, other arithmetic  30.4 us
    all_to_all x1, blocking collectives, on_device(): lax.all_to_all(mixer_in, 'sp', split_axis=2, concat_axis=1, tiled=True)  18.2 us
    all_to_all x1, waiting for transfers between devices, on_device(): lax.all_to_all(mixer_grad, 'sp', split_axis=2, concat_axis=1, tiled=True)  14.4 us
    all_to_all x1, waiting for transfers between devices, on_device(): lax.all_to_all(normed_back.reshape(sequences, -1, channels), 'sp', split_...  13.5 us
    all_to_all x1, waiting for transfers between devices, on_device(): lax.all_to_all(spatial.reshape(sequences, -1, channels), 'sp', split_axis...  11.9 us
  transfers between devices with their start and end apart: 7, of which 5 were waited for; matrix products, arithmetic and copies ran while one was open for 2% of the time, Pallas kernels for 0%

commit v1 on v0

v1 whole, which is shorter than its diff:
```python
import math

import jax
import jax.numpy as jnp
from jax import lax
from jax.experimental import pallas as pl
from jax.experimental.pallas import tpu as pltpu
from jax.sharding import PartitionSpec as P

GROUP_CH = 128
SPAN = 512
SEG = 64
ROW_STEP = 32

norm_eps = 1e-05
grad_scale = 1.0 / 256.0
root_half = 1.0 / math.sqrt(2.0)
root_twopi = 1.0 / math.sqrt(2.0 * math.pi)

WHOLE = pl.BlockSpec(memory_space=pltpu.VMEM)
SCALAR = pl.BlockSpec(memory_space=pltpu.SMEM)


def normal_cdf(preact):
    return 0.5 * (1.0 + lax.erf(preact * root_half))


def gelu_slope(preact, cdf):
    return cdf + preact * jnp.exp(-0.5 * preact * preact) * root_twopi


def norm_stats(gate):
    gated_act = gate * normal_cdf(gate)
    width = gate.shape[1]
    centered = gated_act - jnp.sum(gated_act, axis=-1, keepdims=True) * (1.0 / width)
    variance = jnp.sum(centered * centered, axis=-1, keepdims=True) * (1.0 / width)
    inverse_std = lax.rsqrt(variance + norm_eps)
    return centered * inverse_std, inverse_std


def row_loop(rows, body):
    def step(at, carry):
        body(pl.ds(pl.multiple_of(at * ROW_STEP, ROW_STEP), ROW_STEP))
        return carry

    lax.fori_loop(0, rows // ROW_STEP, step, 0)


def send_kernel(second_ref, up_ref, gate_ref, grad_ref, gain_ref, send_ref):
    rows = up_ref.shape[0]

    @pl.when(second_ref[0] == 0)
    def _():
        def body(at):
            normed, _ = norm_stats(gate_ref[at, :].astype(jnp.float32))
            send_ref[at, :] = (normed * gain_ref[...]).astype(jnp.bfloat16)

        row_loop(rows, body)

    @pl.when(second_ref[0] != 0)
    def _():
        def body(at):
            up = up_ref[at, :].astype(jnp.float32)
            mixed = grad_ref[at, :].astype(jnp.float32) * (up * normal_cdf(up))
            send_ref[at, :] = mixed.astype(jnp.bfloat16)

        row_loop(rows, body)


def own_kernel(
    up_ref, gate_ref, grad_ref, gain_ref, own_mix_ref,
    spatial_ref, back_ref, normed_ref, std_ref, up_slope_ref, gate_slope_ref,
    in_ref, mgrad_ref,
):
    rows, width = up_ref.shape

    def body(at):
        gate = gate_ref[at, :].astype(jnp.float32)
        normed, inverse_std = norm_stats(gate)
        normed_ref[at, :] = normed
        std_ref[at, :] = jnp.broadcast_to(inverse_std, (ROW_STEP, GROUP_CH))
        in_ref[at, :] = (normed * gain_ref[...]).astype(jnp.bfloat16)
        gate_slope_ref[at, :] = gelu_slope(gate, normal_cdf(gate))
        up = up_ref[at, :].astype(jnp.float32)
        grad = grad_ref[at, :].astype(jnp.float32)
        cdf = normal_cdf(up)
        mgrad_ref[at, :] = (grad * (up * cdf)).astype(jnp.bfloat16)
        up_slope_ref[at, :] = grad * gelu_slope(up, cdf)

    row_loop(rows, body)
    row_seg = lax.broadcasted_iota(jnp.int32, (rows, rows), 0) // SEG
    col_seg = lax.broadcasted_iota(jnp.int32, (rows, rows), 1) // SEG
    keep = col_seg <= row_seg
    for g in range(width // GROUP_CH):
        cols = slice(g * GROUP_CH, (g + 1) * GROUP_CH)
        weight = own_mix_ref[g].astype(jnp.float32)
        masked = jnp.where(keep, weight, 0.0).astype(jnp.bfloat16)
        spatial_ref[:, cols] = lax.dot_general(
            masked, in_ref[:, cols], (((1,), (0,)), ((), ())), preferred_element_type=jnp.float32
        )
        back_ref[:, cols] = lax.dot_general(
            masked, mgrad_ref[:, cols], (((0,), (0,)), ((), ())), preferred_element_type=jnp.float32
        )


def finish_kernel(
    second_ref, recv_ref, cross_mix_ref, gain_ref,
    spatial_ref, back_ref, normed_ref, std_ref, up_slope_ref, gate_slope_ref,
    both_ref, extra_ref,
):
    rows, width = recv_ref.shape
    groups = width // GROUP_CH
    first = second_ref[0] == 0
    spatial_share = jnp.where(first, 0.0, 1.0)
    back_share = jnp.where(first, 1.0, 0.0)

    def mix(dims):
        for g in range(groups):
            cols = slice(g * GROUP_CH, (g + 1) * GROUP_CH)
            extra_ref[:, cols] = lax.dot_general(
                cross_mix_ref[g], recv_ref[:, cols], (dims, ((), ())),
                preferred_element_type=jnp.float32,
            )

    @pl.when(first)
    def _():
        mix(((0,), (0,)))

    @pl.when(jnp.logical_not(first))
    def _():
        mix(((1,), (0,)))

    def body(at):
        extra = extra_ref[at, :]
        spatial = (spatial_ref[at, :] + extra * spatial_share).astype(jnp.bfloat16)
        back = (back_ref[at, :] + extra * back_share).astype(jnp.bfloat16)
        both_ref[at, :width] = (up_slope_ref[at, :] * spatial.astype(jnp.float32)).astype(
            jnp.bfloat16
        )
        scaled = back.astype(jnp.float32) * gain_ref[...]
        normed = normed_ref[at, :]
        mean = jnp.sum(scaled, axis=-1, keepdims=True) * (1.0 / width)
        along = jnp.sum(scaled * normed, axis=-1, keepdims=True) * (1.0 / width)
        gated_grad = std_ref[at, :1] * (scaled - mean - normed * along)
        both_ref[at, width:] = (gated_grad * gate_slope_ref[at, :]).astype(jnp.bfloat16)

    row_loop(rows, body)


def contract(first_op, second_op, dims):
    return lax.dot_general(
        first_op, second_op, (dims, ((), ())), preferred_element_type=jnp.float32
    )


def on_device(inputs, up_pre, gate_pre, cotangent, norm_gain, up_weight, gate_weight, mix_weight):
    sequences, rows, width = cotangent.shape
    model_width = inputs.shape[2]
    sp_count = lax.axis_size("sp")
    assert sequences == 1 and SPAN == 2 * rows
    f32 = lambda *shape: jax.ShapeDtypeStruct(shape, jnp.float32)
    bf16 = lambda *shape: jax.ShapeDtypeStruct(shape, jnp.bfloat16)
    up_flat = up_pre.reshape(rows, width)
    gate_flat = gate_pre.reshape(rows, width)
    grad_flat = cotangent.reshape(rows, width)
    gain = norm_gain.reshape(1, width)
    half = lax.axis_index("sp") % 2
    second = half.astype(jnp.int32).reshape(1)

    moved_inputs = lax.all_to_all(
        inputs.reshape(rows, model_width), "dp", split_axis=1, concat_axis=0, tiled=True
    )

    send = pl.pallas_call(
        send_kernel,
        out_shape=bf16(rows, width),
        in_specs=[SCALAR] + [WHOLE] * 4,
        out_specs=WHOLE,
        name="send_half",
    )(second, up_flat, gate_flat, grad_flat, gain)
    recv = lax.ppermute(send, "sp", [(i, i ^ 1) for i in range(sp_count)])

    groups = mix_weight.shape[0]
    own_mix = lax.dynamic_slice(
        mix_weight, (0, half * rows, half * rows), (groups, rows, rows)
    )
    cross_mix = mix_weight[:, rows:, :rows]
    local = pl.pallas_call(
        own_kernel,
        out_shape=(
            f32(rows, width), f32(rows, width), f32(rows, width),
            f32(rows, GROUP_CH), f32(rows, width), f32(rows, width),
        ),
        in_specs=[WHOLE] * 5,
        out_specs=(WHOLE,) * 6,
        scratch_shapes=[pltpu.VMEM((rows, width), jnp.bfloat16)] * 2,
        cost_estimate=pl.CostEstimate(
            flops=20_000_000_000, transcendentals=0, bytes_accessed=8 * 1024 * 1024
        ),
        name="own_half",
    )(up_flat, gate_flat, grad_flat, gain, own_mix)
    both = pl.pallas_call(
        finish_kernel,
        out_shape=bf16(rows, 2 * width),
        in_specs=[SCALAR] + [WHOLE] * 9,
        out_specs=WHOLE,
        scratch_shapes=[pltpu.VMEM((rows, width), jnp.float32)],
        name="finish",
    )(second, recv, cross_mix, gain, *local)

    every = lax.all_gather(both, "dp", axis=0, tiled=True)
    part = contract(moved_inputs, every, ((0,), (0,))).astype(jnp.bfloat16)
    own_part = lax.psum_scatter(part, "sp", scatter_dimension=0, tiled=True)
    weight_rows = lax.all_gather(own_part, "sp", axis=0, tiled=True)

    columns = (
        contract(every[:, :width], up_weight, ((1,), (1,)))
        + contract(every[:, width:], gate_weight, ((1,), (1,)))
    ).astype(jnp.bfloat16)
    input_grad = lax.all_to_all(columns, "dp", split_axis=0, concat_axis=1, tiled=True)
    input_grad = input_grad.reshape(sequences, rows, model_width)
    up_weight_grad = weight_rows[:, :width].astype(jnp.float32) * grad_scale
    gate_weight_grad = weight_rows[:, width:].astype(jnp.float32) * grad_scale
    return (input_grad, up_weight_grad, gate_weight_grad)


def solution(mesh):
    return jax.shard_map(
        on_device,
        mesh=mesh,
        in_specs=(
            P("dp", "sp", None),
            P("dp", "sp", None),
            P("dp", "sp", None),
            P("dp", "sp", None),
            P(),
            P("dp", None),
            P("dp", None),
            P(),
        ),
        out_specs=(P("dp", "sp", None), P("dp", None), P("dp", None)),
        check_vma=False,
    )
```

time: 511 us -> 212 us (0.41)
  waiting for transfers between devices: 338 us -> 114 us
  local copies, waits for them, and re-layouts: 53.9 us -> 10.6 us
  other arithmetic: 42.2 us -> 4.14 us
  blocking collectives: 18.2 us -> 42.1 us
  Pallas kernels: 0 us -> 16.1 us
  starting transfers between devices: 16.8 us -> 1.71 us
  matrix products: 20.4 us -> 9.17 us
    reduce_scatter x1, waiting for transfers between devices: 232 us -> 68 us  [on_device(): own_part = lax.psum_scatter(part, 'sp', scatter_dimension=0, tiled=True)]
    all_to_all x3 -> x0, waiting for transfers between devices: 39.8 us -> none  [the longest x1 14.4 us: on_device(): lax.all_to_all(mixer_grad, 'sp', split_axis=2, concat_axis=1, tiled=True)]
    all_gather x1, waiting for transfers between devices: 65.3 us -> 26.5 us  [on_device(): weight_rows = lax.all_gather(own_part, 'sp', axis=0, tiled=True)]
    unnamed x4 -> x0, other arithmetic: 30.4 us -> none
    unnamed x30 -> x12, local copies, waits for them, and re-layouts: 31.6 us -> 3.78 us
    all_to_all x1 -> x2, blocking collectives: 18.2 us -> 42.1 us  [the longest x1 25.1 us: on_device(): lax.all_to_all(inputs.reshape(rows, model_width), 'dp', split_axis=1, con...]
    all_to_all x3 -> x0, starting transfers between devices: 16.4 us -> none  [the longest x1 7.6 us: on_device(): lax.all_to_all(mixer_grad, 'sp', split_axis=2, concat_axis=1, tiled=True)]
    pallas_call x0 -> x3, Pallas kernels: none -> 16.1 us  [the longest x1 6.21 us: on_device(): pl.pallas_call(own_kernel, out_shape=(f32(rows, width), f32(rows, width),...]
  transfers between devices with their start and end apart: 7 -> 4, of which waited for: 5 -> 4; matrix products, arithmetic and copies ran while one was open for 2% -> 6% of each run, Pallas kernels for 0% -> 3%
where the time goes in v1:
time: 212 us; the launch traced here: 211 us
  waiting for transfers between devices  114 us (54%)
  blocking collectives  42.1 us (20%)
  Pallas kernels  16.1 us (8%)
  between operations  13.8 us (7%)
  local copies, waits for them, and re-layouts  10.6 us (5%)
  matrix products  9.17 us (4%)
  other arithmetic  4.14 us (2%)
    reduce_scatter x1, waiting for transfers between devices, on_device(): own_part = lax.psum_scatter(part, 'sp', scatter_dimension=0, tiled=True)  68 us
    all_gather x1, waiting for transfers between devices, on_device(): weight_rows = lax.all_gather(own_part, 'sp', axis=0, tiled=True)  26.5 us
    all_to_all x1, blocking collectives, on_device(): lax.all_to_all(inputs.reshape(rows, model_width), 'dp', split_axis=1, con...  25.1 us
    all_to_all x1, blocking collectives, on_device(): lax.all_to_all(columns, 'dp', split_axis=0, concat_axis=1, tiled=True)  17 us
    all_gather x1, waiting for transfers between devices, on_device(): every = lax.all_gather(both, 'dp', axis=0, tiled=True)  15.5 us
    dot_general x3, matrix products, contract(): lax.dot_general(first_op, second_op, (dims, ((), ())), preferred_element_...  9.17 us
    pallas_call x1, Pallas kernels, on_device(): pl.pallas_call(own_kernel, out_shape=(f32(rows, width), f32(rows, width),...  6.21 us
    pallas_call x1, Pallas kernels, on_device(): pl.pallas_call(finish_kernel, out_shape=bf16(rows, 2 * width), in_specs=[...  5.92 us
  transfers between devices with their start and end apart: 4, of which 4 were waited for; matrix products, arithmetic and copies ran while one was open for 6% of the time, Pallas kernels for 3%

profile of v1, /device:TPU:0, one launch (start us, length us, event | category | flops | bytes accessed | tf_op | source)
XLA Modules:
  0.0 211.3 jit_solution(5066276352772644979)
XLA Ops:
  7.2 0.0 copy-start
  7.2 0.0 all-gather.3.cloned.1.call-start
  7.2 4.0 %send_half.1 = bf16[256,1024]{1,0:T(8,128)(2,1)} custom-call(s32[1]{0:T(128)} %bitcast.second_ref, bf16[256,1024]{1,0:T(8,128)(2,1)} %bitcast.22, bf16[256,1024]{1,0:T(8,128)(2,1)} %bitcast.24, bf16[256,1024]{1,0:T(8,128)(2,1)} %bitcast.26, f32[1,1024]{1,0:T(1,128)} %bitcast.28), custom_call_target="tpu_custom_call" | custom-call | tf_op jit(solution)/shard_map/send_half/pallas_call | solution.py:174
  11.2 1.6 collective-permute-start
  12.8 3.1 %constant_dynamic-slice_fusion = (bf16[8,256,256]{2,1,0:T(8,128)(2,1)}, bf16[8,256,256]{2,1,0:T(8,128)(2,1)}) fusion(bf16[8,512,512]{2,1,0:T(8,128)(2,1)} %param.15, s32[]{:T(128)S(6)} %select_n.12), kind=kLoop, calls=%fused_computation.9 | loop fusion | bytes 4194308 | tf_op jit(solution)/shard_map/dynamic_slice | solution.py:184
  15.9 6.2 %own_half.1 = (f32[256,1024]{1,0:T(8,128)}, f32[256,1024]{1,0:T(8,128)}, f32[256,1024]{1,0:T(8,128)}, f32[256,128]{1,0:T(8,128)}, f32[256,1024]{1,0:T(8,128)}, /*index=5*/f32[256,1024]{1,0:T(8,128)}) custom-call(bf16[256,1024]{1,0:T(8,128)(2,1)} %bitcast.23, bf16[256,1024]{1,0:T(8,128)(2,1)} %bitcast.25, bf16[256,1024]{1,0:T(8,128)(2,1)} %bitcast.27, ...), custom_call_target="tpu_custom_call" | custom-call | flops 20000000000 | bytes 8388608 | tf_op jit(solution)/shard_map/own_half/pallas_call | solution.py:188
  22.1 3.6 %collective-permute-done.recv_ref = bf16[256,1024]{1,0:T(8,128)(2,1)S(1)} collective-permute-done((bf16[256,1024]{1,0:T(8,128)(2,1)}, bf16[256,1024]{1,0:T(8,128)(2,1)S(1)}, u32[]{:S(2)}, u32[]{:S(2)}) %collective-permute-start) | collective-permute-done | bytes 524320 | tf_op jit(solution)/shard_map/ppermute | solution.py:181
  25.7 0.0 copy-start.2
  25.7 0.8 copy-done.2
  26.5 0.0 copy-start.1
  26.5 5.9 %finish.1 = bf16[256,2048]{1,0:T(8,128)(2,1)} custom-call(s32[1]{0:T(128)} %bitcast.second_ref, bf16[256,1024]{1,0:T(8,128)(2,1)} %copy-done.2, bf16[8,256,256]{2,1,0:T(8,128)(2,1)} %get-tuple-element.25.cross_mix_ref, f32[1,1024]{1,0:T(1,128)} %bitcast.30, f32[256,1024]{1,0:T(8,128)} %get-tuple-element.9.spatial_ref, ...), custom_call_target="tpu_custom_call" | custom-call | tf_op jit(solution)/shard_map/finish/pallas_call | solution.py:202
  32.4 0.0 all-gather.3.cloned.1.call-update
  32.5 0.0 reduce-scatter.4.cloned.1.call-start
  32.5 0.0 copy-done.1
  32.5 0.5 copy.23
  33.1 25.1 %all_to_all.35 = bf16[256,4,512]{0,2,1:T(8,128)(2,1)S(1)} all-to-all(bf16[256,4,512]{0,2,1:T(8,128)(2,1)S(1)} %bitcast.19), channel_id=1, replica_groups=mesh['sp'=8,'dp'=4] {'dp'}, dimensions={1} | all-to-all | bytes 2097152 | tf_op jit(solution)/shard_map/all_to_all | solution.py:170
  58.2 1.3 copy.24
  59.5 15.5 %all-gather.3.cloned.1.call-done = bf16[1024,2048]{1,0:T(8,128)(2,1)} async-done(((bf16[256,2048]{1,0:T(8,128)(2,1)}), bf16[1024,2048]{1,0:T(8,128)(2,1)}) %all-gather.3.cloned.1.call-update) | async-done | bytes 4194320 | tf_op jit(solution)/shard_map/all_gather | solution.py:211
  75.0 4.9 %fusion = bf16[512,2048]{0,1:T(8,128)(2,1)S(1)} fusion(bf16[1024,2048]{1,0:T(8,128)(2,1)} %all-gather.3.cloned.1.call-done, bf16[1024,512]{1,0:T(8,128)(2,1)} %bitcast.20), kind=kOutput, calls=%fused_computation.1 | convolution fusion | flops 2148532224 | bytes 7340032 | tf_op jit(solution)/shard_map/dot_general | solution.py:151
  79.9 2.4 %copy.26 = bf16[512,2048]{1,0:T(8,128)(2,1)} copy(bf16[512,2048]{0,1:T(8,128)(2,1)S(1)} %fusion) | data formatting | bytes 4194304
  82.2 0.0 reduce-scatter.4.cloned.1.call-update
  82.3 0.0 all-gather.5.cloned.1.call-start
  82.3 68.0 %reduce-scatter.4.cloned.1.call-done = bf16[64,2048]{1,0:T(8,128)(2,1)} async-done(((bf16[512,2048]{1,0:T(8,128)(2,1)}), bf16[64,2048]{1,0:T(8,128)(2,1)}) %reduce-scatter.4.cloned.1.call-update) | async-done | bytes 262160 | tf_op jit(solution)/shard_map/reduce_scatter | solution.py:213
  150.3 0.0 all-gather.5.cloned.1.call-update
  150.3 0.0 copy-done
  150.3 0.0 copy-start.3
  150.3 0.0 copy-start.4
  150.4 3.0 %fusion.1 = f32[1024,512]{1,0:T(8,128)S(1)} fusion(bf16[512,1024]{1,0:T(8,128)(2,1)S(1)} %copy-done, bf16[1024,2048]{1,0:T(8,128)(2,1)} %all-gather.3.cloned.1.call-done), kind=kOutput, calls=%fused_computation.2 | convolution fusion | flops 1073741824 | bytes 5242880 | tf_op jit(solution)/shard_map/dot_general | solution.py:151
  153.4 0.0 copy-done.3
  153.4 0.1 copy-done.4
  153.4 1.3 add_convert_fusion
  154.7 17.0 %all_to_all.36 = bf16[4,256,512]{2,1,0:T(8,128)(2,1)S(1)} all-to-all(bf16[4,256,512]{2,1,0:T(8,128)(2,1)S(1)} %bitcast.21), channel_id=1, replica_groups=mesh['sp'=8,'dp'=4] {'dp'}, dimensions={0} | all-to-all | bytes 2097152 | tf_op jit(solution)/shard_map/all_to_all | solution.py:220
  171.7 0.8 copy.22
  172.5 1.6 reshape.38
  174.1 26.5 %all-gather.5.cloned.1.call-done = bf16[512,2048]{1,0:T(8,128)(2,1)} async-done(((bf16[64,2048]{1,0:T(8,128)(2,1)}), bf16[512,2048]{1,0:T(8,128)(2,1)}) %all-gather.5.cloned.1.call-update) | async-done | bytes 2097168 | tf_op jit(solution)/shard_map/all_gather | solution.py:214
  200.6 4.1 %convert_multiply_fusion = (f32[512,1024]{1,0:T(8,128)}, f32[512,1024]{1,0:T(8,128)}) fusion(bf16[512,2048]{1,0:T(8,128)(2,1)} %all-gather.5.cloned.1.call-done), kind=kLoop, calls=%fused_computation.6 | loop fusion | flops 2097152 | bytes 6291456 | tf_op jit(solution)/shard_map/mul | solution.py:223
Async XLA Ops:
  7.2 143.2 %copy-start = (bf16[512,1024]{1,0:T(8,128)(2,1)S(1)}, bf16[512,1024]{1,0:T(8,128)(2,1)}, u32[]{:S(2)}) copy-start(bf16[512,1024]{1,0:T(8,128)(2,1)} %param.14) | copy-start | bytes 3145732
  7.2 67.8 %all-gather.3.cloned.1.call-start = ((), (), s32[]{:S(2)}) async-start(), calls=%async_computation.3 | async-start | bytes 5242880 | tf_op jit(solution)/shard_map/all_gather | solution.py:211
  11.2 14.5 %collective-permute-start = (bf16[256,1024]{1,0:T(8,128)(2,1)}, bf16[256,1024]{1,0:T(8,128)(2,1)S(1)}, u32[]{:S(2)}, u32[]{:S(2)}) collective-permute-start(bf16[256,1024]{1,0:T(8,128)(2,1)} %send_half.1), channel_id=1, source_target_pairs={{0,4},{4,0},{8,12},{12,8},{16,20},{20,16},{24,28},{28,24},{1,5},{5... | collective-permute-start | bytes 1572872 | tf_op jit(solution)/shard_map/ppermute | solution.py:181
  25.7 0.8 copy-start.2
  26.5 6.0 %copy-start.1 = (bf16[1,256,2048]{2,1,0:T(8,128)(2,1)S(1)}, bf16[1,256,2048]{2,1,0:T(8,128)(2,1)}, u32[]{:S(2)}) copy-start(bf16[1,256,2048]{2,1,0:T(8,128)(2,1)} %param.8) | copy-start | bytes 3145732
  32.5 117.8 %reduce-scatter.4.cloned.1.call-start = ((), (), s32[]{:S(2)}) async-start(), calls=%async_computation.5 | async-start | bytes 2359296 | tf_op jit(solution)/shard_map/reduce_scatter | solution.py:213
  82.3 118.3 %all-gather.5.cloned.1.call-start = ((), (), s32[]{:S(2)}) async-start(), calls=%async_computation.4 | async-start | bytes 2359296 | tf_op jit(solution)/shard_map/all_gather | solution.py:214
  150.3 3.1 %copy-start.3 = (bf16[1024,2048]{1,0:T(8,128)(2,1)S(1)}, bf16[1024,2048]{1,0:T(8,128)(2,1)}, u32[]{:S(2)}) copy-start(bf16[1024,2048]{1,0:T(8,128)(2,1)} %all-gather.3.cloned.1.call-done) | copy-start | bytes 12582916
  150.3 3.1 %copy-start.4 = (bf16[512,1024]{1,0:T(8,128)(2,1)S(1)}, bf16[512,1024]{1,0:T(8,128)(2,1)}, u32[]{:S(2)}) copy-start(bf16[512,1024]{1,0:T(8,128)(2,1)} %param.13) | copy-start | bytes 3145732
Sparse Core Ops, SparseCore 0:
  32.6 42.3 all-gather.2
  82.4 67.8 reduce-scatter.3
  152.4 48.1 all-gather.4
